TPU v7x, 32 devices: a whole 2x2x4 slice. The times are simulated.
32 devices in a mesh: sp: 4 (over z), fs: 4 (over y, x), tp: 2 (over core).
Axes of the slice: x: 2, y: 2, z: 4, core: 2. Of those that a mesh axis runs over, the one named last changes fastest.
Arguments:
- tokens: bfloat16 [4, 1024, 2048], P('fs', 'sp', 'tp'), may hold values from -6 to 6
- norm_gain: float32 [2048], replicated, may hold values from 0.1 to 1.9
- ret_query: bfloat16 [2048, 1024], P('sp', 'tp'), may hold values from -0.125 to 0.125
- ret_key: bfloat16 [2048, 1024], P('sp', 'tp'), may hold values from -0.125 to 0.125
- ret_value: bfloat16 [2048, 1024], P('sp', 'tp'), may hold values from -0.125 to 0.125
- att_query: bfloat16 [2048, 1024], P('sp', 'tp'), may hold values from -0.125 to 0.125
- att_key: bfloat16 [2048, 256], P('sp', 'tp'), may hold values from -0.125 to 0.125
- att_value: bfloat16 [2048, 256], P('sp', 'tp'), may hold values from -0.125 to 0.125
- log_decay: float32 [4, 4, 1024], P('fs', 'tp', 'sp'), may hold values from -1 to 0
- start_state: float32 [4, 4, 256, 256], P('fs', 'tp'), may hold values from -12 to 12
- ret_gain: float32 [1024], P('tp'), may hold values from 0.1 to 1.9
- sink_logits: float32 [16], P('tp'), may hold values from 1 to 5
- ret_out: bfloat16 [1024, 2048], P('tp', 'fs'), may hold values from -0.1875 to 0.1875
- att_out: bfloat16 [1024, 2048], P('tp', 'fs'), may hold values from -1.5 to 1.5
Outputs:
- mixed: bfloat16 [4, 1024, 2048], P('fs', 'sp', 'tp')
All inputs are finite; a program needn't handle non-finite values.
Results may differ from a plain program's by a relative error of at most 0.015.
Values may be sent and summed in bfloat16 or wider, within the bound.
A program may use at most 128 MiB of HBM per device.

v0:
```python
import jax
import jax.numpy as jnp
from jax import lax
from jax.sharding import PartitionSpec as P

DK = 256
DV = 256
HD = 64
WINDOW = 128
BLOCK = 128
epsilon = 1e-06
exact_result = lax.Precision.HIGHEST


def carried_in(array, axis, combine, identity):
    peers, mine = (lax.axis_size(axis), lax.axis_index(axis))
    everything = jax.tree.map(
        lambda part, kind: lax.all_gather(part.astype(kind), axis),
        array,
        (jnp.bfloat16, jnp.bfloat16),
    )
    start = jax.tree.map(
        lambda part, zero: jnp.broadcast_to(jnp.asarray(zero, part.dtype), part.shape),
        array,
        identity,
    )

    def hop(k, before):
        reached = k < mine
        new = combine(
            before, jax.tree.map(lambda part, own: part[k].astype(own.dtype), everything, array)
        )
        return jax.tree.map(lambda a, b: jnp.where(reached, a, b), new, before)

    return lax.fori_loop(0, peers, hop, start)


def passed_along(block, axis, distance):
    devices = range(lax.axis_size(axis))
    route = [(i - distance, i) for i in devices if i - distance in devices]
    return lax.ppermute(block, axis, route)


def rotate(values, positions):
    half_dim = values.shape[-1] // 2
    inverse = 1.0 / 10000.0 ** (jnp.arange(half_dim, dtype=jnp.float32) / half_dim)
    angles = positions.astype(jnp.float32)[:, None] * inverse[None, :]
    cosine = jnp.cos(angles)[:, None, :]
    sine_table = jnp.sin(angles)[:, None, :]
    front_half = values[..., :half_dim]
    back_half = values[..., half_dim:]
    return jnp.concatenate(
        [
            front_half * cosine - back_half * sine_table,
            front_half * sine_table + back_half * cosine,
        ],
        axis=-1,
    )


def block_step(memory_state, inputs):
    queries, key_matrix_rows, value_matrix_rows, log_rates = inputs
    length_here = log_rates.shape[-1]
    causal = jnp.arange(length_here)[:, None] >= jnp.arange(length_here)[None, :]
    running_totals = jnp.cumsum(log_rates, axis=-1)
    relative = running_totals[:, :, None] - running_totals[:, None, :]
    weight = jnp.where(causal[None], jnp.exp(jnp.where(causal[None], relative, 0.0)), 0.0)
    score_matrix = (
        jnp.einsum("hqd,hkd->hqk", queries, key_matrix_rows, precision=exact_result) * weight
    )
    carried_state = jnp.einsum(
        "hqd,hdv->hqv",
        queries * jnp.exp(running_totals)[:, :, None],
        memory_state,
        precision=exact_result,
    )
    output_rows = (
        jnp.einsum("arf,afu->aru", score_matrix, value_matrix_rows, precision=exact_result)
        + carried_state
    )
    decay_factors = jnp.exp(running_totals[:, -1:] - running_totals)
    memory_state = memory_state * jnp.exp(running_totals[:, -1])[:, None, None] + jnp.einsum(
        "iwj,iwe->ije",
        key_matrix_rows * decay_factors[:, :, None],
        value_matrix_rows,
        precision=exact_result,
    )
    return (memory_state, output_rows)


def chain(earlier, later):
    return (earlier[0] * later[0], earlier[1] * later[0][:, None, None] + later[1])


def shards(
    tokens,
    norm_gain,
    ret_query,
    ret_key,
    ret_value,
    att_query,
    att_key,
    att_value,
    log_decay,
    start_state,
    ret_gain,
    sink_logits,
    ret_out,
    att_out,
):
    gathered = lax.all_gather(tokens[0], "tp", axis=1, tiled=True)
    row_count = gathered.shape[0]
    as_float = gathered.astype(jnp.float32)
    normed = (
        as_float
        * lax.rsqrt(jnp.mean(as_float * as_float, axis=-1, keepdims=True) + epsilon)
        * norm_gain
    ).astype(jnp.bfloat16)
    offset = lax.axis_index("sp") * row_count
    positions = offset + jnp.arange(row_count, dtype=jnp.int32)
    weights = (ret_query, ret_key, ret_value, att_query, att_key, att_value)
    pieces = (
        lax.all_gather(weights[0], "sp", axis=0, tiled=True),
        lax.all_gather(weights[1], "sp", axis=0, tiled=True),
        lax.all_gather(weights[2], "sp", axis=0, tiled=True),
        lax.all_gather(weights[3], "sp", axis=0, tiled=True),
        lax.all_gather(weights[4], "sp", axis=0, tiled=True),
        lax.all_gather(weights[5], "sp", axis=0, tiled=True),
    )
    projected = tuple(
        (jnp.dot(normed, piece, preferred_element_type=jnp.float32) for piece in pieces)
    )
    rounded = tuple((product_f.astype(jnp.bfloat16) for product_f in projected))
    projected = rounded[:3]
    head_count = projected[0].shape[1] // DK
    queries = rotate(projected[0].astype(jnp.float32).reshape(row_count, head_count, DK), positions)
    keys_rot = rotate(
        projected[1].astype(jnp.float32).reshape(row_count, head_count, DK), positions
    ) * DK ** (-0.5)
    values_f = projected[2].astype(jnp.float32).reshape(row_count, head_count, DV)
    log_rates = log_decay[0]
    count = row_count // BLOCK

    def blocked(array):
        return array.reshape(count, BLOCK, head_count, array.shape[-1]).transpose(0, 2, 1, 3)

    rates_blocked = log_rates.reshape(head_count, count, BLOCK).transpose(1, 0, 2)
    local_state, pieces = lax.scan(
        block_step,
        jnp.zeros((head_count, DK, DV), jnp.float32),
        (blocked(queries), blocked(keys_rot), blocked(values_f), rates_blocked),
    )
    local_out = pieces.transpose(0, 2, 1, 3).reshape(row_count, head_count, DV)
    running_totals = jnp.cumsum(log_rates, axis=-1)
    device_decay = jnp.exp(running_totals[:, -1])
    identity = (jnp.ones((head_count,), jnp.float32), jnp.zeros((head_count, DK, DV), jnp.float32))
    prior_decay, prior_state = carried_in((device_decay, local_state), "sp", chain, identity)
    incoming = prior_state + prior_decay[:, None, None] * start_state[0]
    retained = local_out + jnp.einsum(
        "thd,hdv->thv",
        queries * jnp.exp(running_totals).T[:, :, None],
        incoming,
        precision=exact_result,
    )
    centred = retained - jnp.mean(retained, axis=-1, keepdims=True)
    variance = jnp.mean(centred * centred, axis=-1, keepdims=True)
    ret_hidden = (
        (centred * lax.rsqrt(variance + epsilon)).reshape(row_count, head_count * DV) * ret_gain
    ).astype(jnp.bfloat16)
    att_queries, att_keys, att_values = rounded[3:]
    kv_heads = att_keys.shape[1] // HD
    groups = att_queries.shape[1] // HD // kv_heads
    earlier_keys, earlier_values = passed_along(
        (att_keys[row_count - WINDOW :], att_values[row_count - WINDOW :]), "sp", 1
    )
    extended_keys = jnp.concatenate([earlier_keys, att_keys], axis=0)
    extended_values = jnp.concatenate([earlier_values, att_values], axis=0)
    windows = row_count // WINDOW

    def banded(array):
        earlier = array[:row_count].reshape(windows, WINDOW, kv_heads, HD)
        current = array[WINDOW:].reshape(windows, WINDOW, kv_heads, HD)
        return jnp.concatenate([earlier, current], axis=1)

    key_band = banded(extended_keys)
    value_band = banded(extended_values)
    grouped_q = att_queries.reshape(windows, WINDOW, kv_heads, groups, HD)
    score_matrix = jnp.einsum(
        "nqhgd,nkhd->nhgqk", grouped_q, key_band, preferred_element_type=jnp.float32
    ) * HD ** (-0.5)
    query_index = WINDOW + jnp.arange(WINDOW)
    key_index = jnp.arange(2 * WINDOW)
    allowed = (key_index[None, :] <= query_index[:, None]) & (
        query_index[:, None] - key_index[None, :] < WINDOW
    )
    key_place = offset - WINDOW + jnp.arange(windows)[:, None] * WINDOW + key_index[None, :]
    visible = (allowed[None] & (key_place >= 0)[:, None, :])[:, None, None]
    expo = jnp.exp(jnp.where(visible, score_matrix, -1e30))
    summed = jnp.sum(expo, axis=-1, keepdims=True) + jnp.exp(sink_logits).reshape(
        1, kv_heads, groups, 1, 1
    )
    probs = (expo / summed).astype(jnp.bfloat16)
    attended = jnp.einsum(
        "nhgqk,nkhd->nqhgd", probs, value_band, preferred_element_type=jnp.float32
    )
    att_hidden = attended.astype(jnp.bfloat16).reshape(row_count, kv_heads * groups * HD)
    ret_width = ret_hidden.shape[1]
    joined = jnp.concatenate([ret_hidden, att_hidden], axis=1)[None]
    piece = lax.all_gather(joined, "fs", axis=0, tiled=True)
    product = jnp.einsum(
        "srh,hd->srd", piece[:, :, :ret_width], ret_out, preferred_element_type=jnp.float32
    )
    product = product + jnp.einsum(
        "srh,hd->srd", piece[:, :, ret_width:], att_out, preferred_element_type=jnp.float32
    )
    partial_rows = product.astype(jnp.bfloat16)
    regrouped = lax.all_to_all(partial_rows, "fs", split_axis=0, concat_axis=2, tiled=True)
    mixed = lax.psum_scatter(
        regrouped[0].astype(jnp.float32).astype(jnp.bfloat16), "tp", scatter_dimension=1, tiled=True
    )
    return mixed[None]


def solution(mesh):
    placed = (
        P("fs", "sp", "tp"),
        P(),
        P("sp", "tp"),
        P("sp", "tp"),
        P("sp", "tp"),
        P("sp", "tp"),
        P("sp", "tp"),
        P("sp", "tp"),
        P("fs", "tp", "sp"),
        P("fs", "tp", None, None),
        P("tp"),
        P("tp"),
        P("tp", "fs"),
        P("tp", "fs"),
    )
    return jax.shard_map(
        shards, mesh=mesh, in_specs=placed, out_specs=P("fs", "sp", "tp"), check_vma=False
    )
```

profile of v0, /device:TPU:0, one launch (start us, length us, event | category | flops | bytes accessed | tf_op | source)
XLA Modules:
  0.0 330.0 jit_solution(6295431087866726067)
XLA Ops:
  13.0 13.6 %all-reduce = bf16[8]{0:T(256)(128)(2,1)S(1)} all-reduce(bf16[8]{0:T(256)(128)(2,1)S(1)} %dynamic-update-slice), channel_id=3, replica_groups=mesh['sp'=4,'fs'=4,'tp'=2] {'sp'}, use_global_device_ids=true, to_apply=%add | all-reduce | flops 8 | bytes 32
  26.6 18.4 %all_gather.42 = bf16[2048,128]{1,0:T(8,128)(2,1)S(1)} all-gather(bf16[512,128]{1,0:T(8,128)(2,1)S(1)} %copy-done.12), channel_id=1, replica_groups=mesh['sp'=4,'fs'=4,'tp'=2] {'sp'}, dimensions={0}, use_global_device_ids=true | all-gather | bytes 655360 | tf_op jit(solution)/shard_map/all_gather | solution.py:127
  45.7 21.2 %all_gather.41 = bf16[2048,128]{1,0:T(8,128)(2,1)} all-gather(bf16[512,128]{1,0:T(8,128)(2,1)S(1)} %copy-done.13), channel_id=1, replica_groups=mesh['sp'=4,'fs'=4,'tp'=2] {'sp'}, dimensions={0}, use_global_device_ids=true | all-gather | bytes 655360 | tf_op jit(solution)/shard_map/all_gather | solution.py:128
  68.9 1.6 fusion.25
  70.5 1.7 convolution_convert_fusion.5
  72.9 2.6 collective-permute-start.1
  75.5 5.5 %all-gather.12.cloned.1.call-done = bf16[2048,512]{1,0:T(8,128)(2,1)} async-done(((bf16[512,512]{1,0:T(8,128)(2,1)}), bf16[2048,512]{1,0:T(8,128)(2,1)}) %all-gather.12.cloned.1.call-update) | async-done | bytes 2097168 | tf_op jit(solution)/shard_map/all_gather | solution.py:124
  80.9 2.3 fusion.31
  83.6 44.0 %all-gather.16.cloned.1.call-done = bf16[2048,512]{1,0:T(8,128)(2,1)} async-done(((bf16[512,512]{1,0:T(8,128)(2,1)}), bf16[2048,512]{1,0:T(8,128)(2,1)}) %all-gather.16.cloned.1.call-update) | async-done | bytes 2097168 | tf_op jit(solution)/shard_map/all_gather | solution.py:123
  127.6 2.7 fusion.33
  131.4 42.1 %all-gather.14.cloned.1.call-done = bf16[2048,512]{1,0:T(8,128)(2,1)} async-done(((bf16[512,512]{1,0:T(8,128)(2,1)}), bf16[2048,512]{1,0:T(8,128)(2,1)}) %all-gather.14.cloned.1.call-update) | async-done | bytes 2097168 | tf_op jit(solution)/shard_map/all_gather | solution.py:125
  173.6 2.7 fusion.32
  178.9 6.7 %while.29 = (s32[]{:T(128)}, f32[2,256,256]{2,1,0:T(8,128)S(1)}, f32[2,2,128,256]{3,2,1,0:T(8,128)}, f32[2,2,128]{2,1,0:T(2,128)S(1)}, f32[2,2,128,256]{3,2,0,1:...) while((s32[]{:T(128)}, f32[2,256,256]{2,1,0:T(8,128)S(1)}, ...), condition=%wide.region_3.4_spmd.clone, body=%wide.region_1.3_spmd.clone.sunk | while | flops 604880896 | bytes 4242084 | solution.py:148
  186.4 1.9 convolution_convert_fusion.6
  188.6 2.3 collective-permute-start
  194.9 24.5 %all-gather.18.cloned.1.call-done = bf16[2048,512]{1,0:T(8,128)(2,1)} async-done(((bf16[512,512]{1,0:T(8,128)(2,1)}), bf16[2048,512]{1,0:T(8,128)(2,1)}) %all-gather.18.cloned.1.call-update) | async-done | bytes 2097168 | tf_op jit(solution)/shard_map/all_gather | solution.py:126
  219.5 2.3 convolution_convert_fusion.1
  223.8 25.1 %all-gather.22.cloned.1.call-done = bf16[8,256,256]{2,1,0:T(8,128)(2,1)} async-done(((bf16[2,256,256]{2,1,0:T(8,128)(2,1)}), bf16[8,256,256]{2,1,0:T(8,128)(2,1)}) %all-gather.22.cloned.1.call-update) | async-done | bytes 1048592 | tf_op jit(solution)/shard_map/all_gather | solution.py:18
  248.9 4.6 %while.30 = (s32[]{:T(128)}, f32[2]{0:T(128)S(1)}, f32[2,256,256]{2,1,0:T(8,128)S(1)}, s32[]{:T(128)}, bf16[4,2]{1,0:T(4,128)(2,1)S(1)}, /*index=5*/bf16[4,2,256,256]{3,2,1,0:T(8,128)(2,1)}, s32[]{:T(128)}, s32[]{:T(128)}) while((s32[]{:T(128)}, f32[2]{0:T(128)S(1)}, f32[2,256,256]{2,1,0:T(8,128)S(1)}, s32[]{:T(128)}, ...), condition=%wide.region_7.8_spmd.clone, body=%wide.region_6.7_spmd.clone.sunk | while | flops 655372 | bytes 1310871 | solution.py:35
  255.9 34.5 %all-gather.24.cloned.1.call-done = bf16[1024,1024]{0,1:T(8,128)(2,1)} async-done(((bf16[256,1024]{0,1:T(8,128)(2,1)}), bf16[1024,1024]{0,1:T(8,128)(2,1)}) %all-gather.24.cloned.1.call-update) | async-done | bytes 2097168 | tf_op jit(solution)/shard_map/all_gather | solution.py:209
  290.4 2.9 copy.81
  295.1 16.7 %all_to_all.15 = bf16[4,256,512]{2,1,0:T(8,128)(2,1)S(1)} all-to-all(bf16[4,256,512]{2,1,0:T(8,128)(2,1)S(1)} %add_convert_fusion), channel_id=1, replica_groups=mesh['sp'=4,'fs'=4,'tp'=2] {'fs'}, dimensions={0} | all-to-all | bytes 2097152 | tf_op jit(solution)/shard_map/all_to_all | solution.py:217
  313.1 8.0 %reduce-scatter.2.cloned.1.call-done = bf16[256,1024]{0,1:T(8,128)(2,1)} async-done(((bf16[256,2048]{0,1:T(8,128)(2,1)}), bf16[256,1024]{0,1:T(8,128)(2,1)}) %reduce-scatter.2.cloned.1.call-update) | async-done | bytes 524304 | tf_op jit(solution)/shard_map/reduce_scatter | solution.py:218
  321.1 2.0 copy.83
  (162 shorter events, 36.5 us)
Async XLA Ops:
  6.5 286.8 %copy-start = (bf16[512,512]{1,0:T(8,128)(2,1)S(1)}, bf16[512,512]{1,0:T(8,128)(2,1)}, u32[]{:S(2)}) copy-start(bf16[512,512]{1,0:T(8,128)(2,1)} %param.30) | copy-start | bytes 1572868
  6.5 4.8 %copy-start.23 = (u32[32]{0:T(128)S(1)}, u32[32]{0:T(128)}, u32[]{:S(2)}) copy-start(u32[32]{0:T(128)} %constant.93) | copy-start | bytes 388
  6.5 20.1 %copy-start.12 = (bf16[512,128]{1,0:T(8,128)(2,1)S(1)}, bf16[512,128]{1,0:T(8,128)(2,1)}, u32[]{:S(2)}) copy-start(bf16[512,128]{1,0:T(8,128)(2,1)} %param.24) | copy-start | bytes 393220
  6.5 38.6 %copy-start.22 = (f32[8]{0:T(128)S(1)}, f32[8]{0:T(128)}, u32[]{:S(2)}) copy-start(f32[8]{0:T(128)} %param.29) | copy-start | bytes 100
  6.5 39.2 %copy-start.13 = (bf16[512,128]{1,0:T(8,128)(2,1)S(1)}, bf16[512,128]{1,0:T(8,128)(2,1)}, u32[]{:S(2)}) copy-start(bf16[512,128]{1,0:T(8,128)(2,1)} %param.25) | copy-start | bytes 393220
  6.6 62.3 %all-gather.20.cloned.1.call-start = ((), (), s32[]{:S(2)}) async-start(), calls=%async_computation.7 | async-start | bytes 1572864 | tf_op jit(solution)/shard_map/all_gather | solution.py:111
  7.3 73.6 %all-gather.12.cloned.1.call-start = ((), (), s32[]{:S(2)}) async-start(), calls=%async_computation.2 | async-start | bytes 2621440 | tf_op jit(solution)/shard_map/all_gather | solution.py:124
  8.0 62.5 %copy-start.20 = (f32[2048]{0:T(1024)S(1)}, f32[2048]{0:T(1024)}, u32[]{:S(2)}) copy-start(f32[2048]{0:T(1024)} %param.19) | copy-start | bytes 24580
  8.1 119.6 %all-gather.16.cloned.1.call-start = ((), (), s32[]{:S(2)}) async-start(), calls=%async_computation.4 | async-start | bytes 2621440 | tf_op jit(solution)/shard_map/all_gather | solution.py:123
  8.8 164.8 %all-gather.14.cloned.1.call-start = ((), (), s32[]{:S(2)}) async-start(), calls=%async_computation.3 | async-start | bytes 2621440 | tf_op jit(solution)/shard_map/all_gather | solution.py:125
  9.4 210.1 %all-gather.18.cloned.1.call-start = ((), (), s32[]{:S(2)}) async-start(), calls=%async_computation.5 | async-start | bytes 2621440 | tf_op jit(solution)/shard_map/all_gather | solution.py:126
  10.0 238.9 %all-gather.22.cloned.1.call-start = ((), (), s32[]{:S(2)}) async-start(), calls=%async_computation.8 | async-start | bytes 1310720 | tf_op jit(solution)/shard_map/all_gather | solution.py:18
  68.9 12.1 %copy-start.5 = (bf16[1,256,2048]{2,1,0:T(8,128)(2,1)S(1)}, bf16[1,256,2048]{2,1,0:T(8,128)(2,1)}, u32[]{:S(2)}) copy-start(bf16[1,256,2048]{2,1,0:T(8,128)(2,1)} %all-gather.20.cloned.1.call-done) | copy-start | bytes 3145732
  70.5 103.1 %copy-start.18 = (f32[256]{0:T(256)}, f32[256]{0:T(256)S(1)}, u32[]{:S(2)}) copy-start(f32[256]{0:T(256)S(1)} %add_rsqrt_fusion.1) | copy-start | bytes 3076
  72.2 11.0 %copy-start.10 = (bf16[256,128]{1,0:T(8,128)(2,1)}, bf16[256,128]{1,0:T(8,128)(2,1)S(1)}, u32[]{:S(2)}) copy-start(bf16[256,128]{1,0:T(8,128)(2,1)S(1)} %convolution_convert_fusion.5) | copy-start | bytes 196612
  72.9 118.2 %collective-permute-start.1 = (bf16[128,128]{1,0:T(8,128)(2,1)}, bf16[128,128]{1,0:T(8,128)(2,1)}, u32[]{:S(2)}, u32[]{:S(2)}) collective-permute-start(bf16[128,128]{1,0:T(8,128)(2,1)} %slice.64), channel_id=1, source_target_pairs={{0,8},{8,16},{16,24},{1,9},{9,17},{17,25},{2,10},{10,18},{18,26},{... | collective-permute-start | bytes 98312 | tf_op jit(solution)/shard_map/ppermute | solution.py:41
  178.8 7.6 %copy-start.19 = (f32[256]{0:T(256)S(1)}, f32[256]{0:T(256)}, u32[]{:S(2)}) copy-start(f32[256]{0:T(256)} %copy-done.18) | copy-start | bytes 3076
  178.8 7.6 %copy-start.21 = (f32[2048]{0:T(1024)S(1)}, f32[2048]{0:T(1024)}, u32[]{:S(2)}) copy-start(f32[2048]{0:T(1024)} %param.19) | copy-start | bytes 24580
  186.4 104.1 %all-gather.24.cloned.1.call-start = ((), (), s32[]{:S(2)}) async-start(), calls=%async_computation.9 | async-start | bytes 2621440 | tf_op jit(solution)/shard_map/all_gather | solution.py:209
  188.3 31.2 %copy-start.6 = (bf16[1,256,2048]{2,1,0:T(8,128)(2,1)S(1)}, bf16[1,256,2048]{2,1,0:T(8,128)(2,1)}, u32[]{:S(2)}) copy-start(bf16[1,256,2048]{2,1,0:T(8,128)(2,1)} %all-gather.20.cloned.1.call-done) | copy-start | bytes 3145732
  188.6 4.3 %collective-permute-start = (bf16[128,128]{1,0:T(8,128)(2,1)S(1)}, bf16[128,128]{1,0:T(8,128)(2,1)S(1)}, u32[]{:S(2)}, u32[]{:S(2)}) collective-permute-start(bf16[128,128]{1,0:T(8,128)(2,1)S(1)} %slice.63), channel_id=1, source_target_pairs={{0,8},{8,16},{16,24},{1,9},{9,17},{17,25},{2,10},{10,18},{18,26},{... | collective-permute-start | bytes 98312 | tf_op jit(solution)/shard_map/ppermute | solution.py:41
  194.9 27.2 %copy-start.14 = (pred[2,128,256]{1,2,0:T(8,128)(4,1)S(1)}, pred[2,128,256]{1,2,0:T(8,128)(4,1)}, u32[]{:S(2)}) copy-start(pred[2,128,256]{1,2,0:T(8,128)(4,1)} %broadcast_and_fusion) | copy-start | bytes 196612
  248.9 4.6 %copy-start.9 = (f32[1,2,256,256]{3,2,1,0:T(8,128)S(1)}, f32[1,2,256,256]{3,2,1,0:T(8,128)}, u32[]{:S(2)}) copy-start(f32[1,2,256,256]{3,2,1,0:T(8,128)} %param.27) | copy-start | bytes 1572868
  255.9 65.2 %reduce-scatter.2.cloned.1.call-start = ((), (), s32[]{:S(2)}) async-start(), calls=%async_computation.6 | async-start | bytes 1572864 | tf_op jit(solution)/shard_map/reduce_scatter | solution.py:218
  (10 other events, 21.6 us)
Sparse Core Ops, SparseCore 0:
  8.9 11.7 all-gather.19
  22.3 58.6 all-gather.11
  82.5 45.0 all-gather.15
  129.1 44.4 all-gather.13
  175.0 44.4 all-gather.17
  220.9 27.9 all-gather.21
  256.0 34.4 all-gather.23
  313.2 7.8 reduce-scatter.1
where the time goes:
time: 331 us; the launch traced here: 330 us
  waiting for transfers between devices  188 us (57%)
  blocking collectives  69.8 us (21%)
  matrix products  23 us (7%)
  local copies, waits for them, and re-layouts  16.4 us (5%)
  between operations  14.8 us (4%)
  other arithmetic  12.8 us (4%)
  starting transfers between devices  5.19 us (2%)
    all_gather x1, waiting for transfers between devices, shards(): lax.all_gather(weights[0], 'sp', axis=0, tiled=True)  44 us
    all_gather x1, waiting for transfers between devices, shards(): lax.all_gather(weights[2], 'sp', axis=0, tiled=True)  42.1 us
    all_gather x1, waiting for transfers between devices, shards(): piece = lax.all_gather(joined, 'fs', axis=0, tiled=True)  34.5 us
    all_gather x1, waiting for transfers between devices, carried_in(): lax.all_gather(part.astype(kind), axis)  25.1 us
    all_gather x1, waiting for transfers between devices, shards(): lax.all_gather(weights[3], 'sp', axis=0, tiled=True)  24.5 us
    all_gather x1, blocking collectives, shards(): lax.all_gather(weights[5], 'sp', axis=0, tiled=True)  21.2 us
    all_gather x1, blocking collectives, shards(): lax.all_gather(weights[4], 'sp', axis=0, tiled=True)  18.4 us
    all_to_all x1, blocking collectives, shards(): lax.all_to_all(partial_rows, 'fs', split_axis=0, concat_axis=2, tiled=True)  16.7 us
  transfers between devices with their start and end apart: 10, of which 8 were waited for; matrix products, arithmetic and copies ran while one was open for 11% of the time, Pallas kernels for 0%

commit v1 on v0

--- a/solution.py
+++ b/solution.py
@@ -10,6 +10,27 @@
 BLOCK = 128
 epsilon = 1e-06
 exact_result = lax.Precision.HIGHEST
+
+
+def gather_around(array, axis, dim):
+    length, index, span = (lax.axis_size(axis), lax.axis_index(axis), array.shape[dim])
+    upward = [(i, (i + 1) % length) for i in range(length)]
+    left = [(i, (i - 1) % length) for i in range(length)]
+    out = jnp.zeros((*array.shape[:dim], length * span, *array.shape[dim + 1 :]), array.dtype)
+    out = lax.dynamic_update_slice_in_dim(out, array, index * span, axis=dim)
+    from_left = from_right = array
+    half = length // 2
+    for turn in range(1, half + 1):
+        from_left = lax.ppermute(from_left, axis, upward)
+        out = lax.dynamic_update_slice_in_dim(
+            out, from_left, (index - turn) % length * span, axis=dim
+        )
+        if turn < length - half:
+            from_right = lax.ppermute(from_right, axis, left)
+            out = lax.dynamic_update_slice_in_dim(
+                out, from_right, (index + turn) % length * span, axis=dim
+            )
+    return out
 
 
 def carried_in(array, axis, combine, identity):
@@ -120,7 +141,7 @@
     positions = offset + jnp.arange(row_count, dtype=jnp.int32)
     weights = (ret_query, ret_key, ret_value, att_query, att_key, att_value)
     pieces = (
-        lax.all_gather(weights[0], "sp", axis=0, tiled=True),
+        gather_around(weights[0], "sp", 0),
         lax.all_gather(weights[1], "sp", axis=0, tiled=True),
         lax.all_gather(weights[2], "sp", axis=0, tiled=True),
         lax.all_gather(weights[3], "sp", axis=0, tiled=True),

time: 331 us -> 295 us (0.89)
  waiting for transfers between devices: 188 us -> 121 us
  blocking collectives: 69.8 us -> 85.1 us
  starting transfers between devices: 5.19 us -> 14.4 us
  local copies, waits for them, and re-layouts: 16.4 us -> 22.5 us
    all_gather x1 -> x0, waiting for transfers between devices: 44 us -> none  [shards(): lax.all_gather(weights[0], 'sp', axis=0, tiled=True)]
    all_gather x1, waiting for transfers between devices: 42.1 us -> 9.82 us  [shards(): lax.all_gather(weights[2], 'sp', axis=0, tiled=True)]
    ppermute x0 -> x3, waiting for transfers between devices: none -> 15.7 us  [the longest x2 15.7 us: gather_around(): from_left = lax.ppermute(from_left, axis, upward)]
    unnamed x1, blocking collectives: 13.6 us -> 27.7 us
    ppermute x0 -> x3, starting transfers between devices: none -> 6.15 us  [the longest x2 4.06 us: gather_around(): from_left = lax.ppermute(from_left, axis, upward)]
    all_gather x1, waiting for transfers between devices: 5.46 us -> 0.01 us  [shards(): lax.all_gather(weights[1], 'sp', axis=0, tiled=True)]
    dynamic_update_slice x0 -> x4, local copies, waits for them, and re-layouts: none -> 4.5 us  [the longest x1 1.91 us: gather_around(): lax.dynamic_update_slice_in_dim(out, from_right, (index + turn) % length...]
  transfers between devices with their start and end apart: 10 -> 12, of which waited for: 8 -> 7; matrix products, arithmetic and copies ran while one was open for 11% -> 15% of each run, Pallas kernels for 0% -> 0%
where the time goes in v1:
time: 295 us; the launch traced here: 294 us
  waiting for transfers between devices  121 us (41%)
  blocking collectives  85.1 us (29%)
  matrix products  23 us (8%)
  local copies, waits for them, and re-layouts  22.5 us (8%)
  between operations  14.8 us (5%)
  starting transfers between devices  14.4 us (5%)
  other arithmetic  13.4 us (5%)
    all_gather x1, waiting for transfers between devices, shards(): piece = lax.all_gather(joined, 'fs', axis=0, tiled=True)  34.5 us
    unnamed x1, blocking collectives  27.7 us
    all_gather x1, waiting for transfers between devices, shards(): lax.all_gather(weights[3], 'sp', axis=0, tiled=True)  25.3 us
    all_gather x1, waiting for transfers between devices, carried_in(): lax.all_gather(part.astype(kind), axis)  24.6 us
    all_gather x1, blocking collectives, shards(): lax.all_gather(weights[4], 'sp', axis=0, tiled=True)  21.5 us
    all_gather x1, blocking collectives, shards(): lax.all_gather(weights[5], 'sp', axis=0, tiled=True)  19.2 us
    all_to_all x1, blocking collectives, shards(): lax.all_to_all(partial_rows, 'fs', split_axis=0, concat_axis=2, tiled=True)  16.7 us
    ppermute x2, waiting for transfers between devices, gather_around(): from_left = lax.ppermute(from_left, axis, upward)  15.7 us
  transfers between devices with their start and end apart: 12, of which 7 were waited for; matrix products, arithmetic and copies ran while one was open for 15% of the time, Pallas kernels for 0%

profile of v1, /device:TPU:0, one launch (start us, length us, event | category | flops | bytes accessed | tf_op | source)
XLA Modules:
  0.0 294.3 jit_solution(2188932016409956058)
XLA Ops:
  8.8 3.1 %collective-permute-start = (bf16[512,512]{1,0:T(8,128)(2,1)}, bf16[512,512]{1,0:T(8,128)(2,1)S(1)}, u32[]{:S(2)}, u32[]{:S(2)}) collective-permute-start(bf16[512,512]{1,0:T(8,128)(2,1)} %param.20), channel_id=1, source_target_pairs={{0,8},{8,16},{16,24},{24,0},{1,9},{9,17},{17,25},{25,1},{2,10},{10... | collective-permute-start | bytes 1572872 | tf_op jit(solution)/shard_map/ppermute | solution.py:24
  11.9 2.1 collective-permute-start.1
  17.5 27.7 %all-reduce = bf16[8]{0:T(256)(128)(2,1)S(1)} all-reduce(bf16[8]{0:T(256)(128)(2,1)S(1)} %dynamic-update-slice), channel_id=3, replica_groups=mesh['sp'=4,'fs'=4,'tp'=2] {'sp'}, use_global_device_ids=true, to_apply=%add | all-reduce | flops 8 | bytes 32
  45.3 21.5 %all_gather.38 = bf16[2048,128]{1,0:T(8,128)(2,1)S(1)} all-gather(bf16[512,128]{1,0:T(8,128)(2,1)S(1)} %copy-done.13), channel_id=1, replica_groups=mesh['sp'=4,'fs'=4,'tp'=2] {'sp'}, dimensions={0}, use_global_device_ids=true | all-gather | bytes 655360 | tf_op jit(solution)/shard_map/all_gather | solution.py:148
  70.8 19.2 %all_gather.37 = bf16[2048,128]{1,0:T(8,128)(2,1)} all-gather(bf16[512,128]{1,0:T(8,128)(2,1)S(1)} %copy-done.14), channel_id=1, replica_groups=mesh['sp'=4,'fs'=4,'tp'=2] {'sp'}, dimensions={0}, use_global_device_ids=true | all-gather | bytes 655360 | tf_op jit(solution)/shard_map/all_gather | solution.py:149
  93.0 1.9 constant_dynamic-update-slice_fusion.1
  96.7 15.7 %collective-permute-done.2 = bf16[512,512]{1,0:T(8,128)(2,1)S(1)} collective-permute-done((bf16[512,512]{1,0:T(8,128)(2,1)S(1)}, bf16[512,512]{1,0:T(8,128)(2,1)S(1)}, u32[]{:S(2)}, u32[]{:S(2)}) %collective-permute-start.2) | collective-permute-done | bytes 524320 | tf_op jit(solution)/shard_map/ppermute | solution.py:24
  113.2 2.3 fusion.33
  115.9 1.7 convolution_convert_fusion.5
  118.3 6.4 %collective-permute-start.4 = (bf16[128,128]{1,0:T(8,128)(2,1)}, bf16[128,128]{1,0:T(8,128)(2,1)}, u32[]{:S(2)}, u32[]{:S(2)}) collective-permute-start(bf16[128,128]{1,0:T(8,128)(2,1)} %slice.64), channel_id=1, source_target_pairs={{0,8},{8,16},{16,24},{1,9},{9,17},{17,25},{2,10},{10,18},{18,26},{... | collective-permute-start | bytes 98312 | tf_op jit(solution)/shard_map/ppermute | solution.py:62
  124.7 2.7 fusion.31
  128.5 9.8 %all-gather.13.cloned.1.call-done = bf16[2048,512]{1,0:T(8,128)(2,1)} async-done(((bf16[512,512]{1,0:T(8,128)(2,1)}), bf16[2048,512]{1,0:T(8,128)(2,1)}) %all-gather.13.cloned.1.call-update) | async-done | bytes 2097168 | tf_op jit(solution)/shard_map/all_gather | solution.py:146
  138.3 2.7 fusion.32
  143.6 6.7 %while.29 = (s32[]{:T(128)}, f32[2,256,256]{2,1,0:T(8,128)S(1)}, f32[2,2,128,256]{3,2,1,0:T(8,128)}, f32[2,2,128]{2,1,0:T(2,128)S(1)}, f32[2,2,128,256]{3,2,0,1:...) while((s32[]{:T(128)}, f32[2,256,256]{2,1,0:T(8,128)S(1)}, ...), condition=%wide.region_3.4_spmd.clone, body=%wide.region_1.3_spmd.clone.sunk | while | flops 604880896 | bytes 4242084 | solution.py:169
  151.2 1.9 convolution_convert_fusion.6
  159.0 25.3 %all-gather.15.cloned.1.call-done = bf16[2048,512]{1,0:T(8,128)(2,1)} async-done(((bf16[512,512]{1,0:T(8,128)(2,1)}), bf16[2048,512]{1,0:T(8,128)(2,1)}) %all-gather.15.cloned.1.call-update) | async-done | bytes 2097168 | tf_op jit(solution)/shard_map/all_gather | solution.py:147
  184.3 2.3 convolution_convert_fusion.1
  188.6 24.6 %all-gather.19.cloned.1.call-done = bf16[8,256,256]{2,1,0:T(8,128)(2,1)} async-done(((bf16[2,256,256]{2,1,0:T(8,128)(2,1)}), bf16[8,256,256]{2,1,0:T(8,128)(2,1)}) %all-gather.19.cloned.1.call-update) | async-done | bytes 1048592 | tf_op jit(solution)/shard_map/all_gather | solution.py:39
  213.2 4.6 %while.30 = (s32[]{:T(128)}, f32[2]{0:T(128)S(1)}, f32[2,256,256]{2,1,0:T(8,128)S(1)}, s32[]{:T(128)}, bf16[4,2]{1,0:T(4,128)(2,1)S(1)}, /*index=5*/bf16[4,2,256,256]{3,2,1,0:T(8,128)(2,1)}, s32[]{:T(128)}, s32[]{:T(128)}) while((s32[]{:T(128)}, f32[2]{0:T(128)S(1)}, f32[2,256,256]{2,1,0:T(8,128)S(1)}, s32[]{:T(128)}, ...), condition=%wide.region_7.8_spmd.clone, body=%wide.region_6.7_spmd.clone.sunk | while | flops 655372 | bytes 1310871 | solution.py:56
  220.2 34.5 %all-gather.21.cloned.1.call-done = bf16[1024,1024]{0,1:T(8,128)(2,1)} async-done(((bf16[256,1024]{0,1:T(8,128)(2,1)}), bf16[1024,1024]{0,1:T(8,128)(2,1)}) %all-gather.21.cloned.1.call-update) | async-done | bytes 2097168 | tf_op jit(solution)/shard_map/all_gather | solution.py:230
  254.7 2.9 copy.81
  259.4 16.7 %all_to_all.15 = bf16[4,256,512]{2,1,0:T(8,128)(2,1)S(1)} all-to-all(bf16[4,256,512]{2,1,0:T(8,128)(2,1)S(1)} %add_convert_fusion), channel_id=1, replica_groups=mesh['sp'=4,'fs'=4,'tp'=2] {'fs'}, dimensions={0} | all-to-all | bytes 2097152 | tf_op jit(solution)/shard_map/all_to_all | solution.py:238
  277.4 8.0 %reduce-scatter.2.cloned.1.call-done = bf16[256,1024]{0,1:T(8,128)(2,1)} async-done(((bf16[256,2048]{0,1:T(8,128)(2,1)}), bf16[256,1024]{0,1:T(8,128)(2,1)}) %reduce-scatter.2.cloned.1.call-update) | async-done | bytes 524304 | tf_op jit(solution)/shard_map/reduce_scatter | solution.py:239
  285.4 2.0 copy.83
  (174 shorter events, 44.4 us)
Async XLA Ops:
  6.5 251.1 %copy-start = (bf16[512,512]{1,0:T(8,128)(2,1)S(1)}, bf16[512,512]{1,0:T(8,128)(2,1)}, u32[]{:S(2)}) copy-start(bf16[512,512]{1,0:T(8,128)(2,1)} %param.30) | copy-start | bytes 1572868
  6.5 38.8 %copy-start.13 = (bf16[512,128]{1,0:T(8,128)(2,1)S(1)}, bf16[512,128]{1,0:T(8,128)(2,1)}, u32[]{:S(2)}) copy-start(bf16[512,128]{1,0:T(8,128)(2,1)} %param.24) | copy-start | bytes 393220
  6.5 60.4 %copy-start.24 = (f32[8]{0:T(128)S(1)}, f32[8]{0:T(128)}, u32[]{:S(2)}) copy-start(f32[8]{0:T(128)} %param.29) | copy-start | bytes 100
  6.5 88.4 %all-gather.17.cloned.1.call-start = ((), (), s32[]{:S(2)}) async-start(), calls=%async_computation.6 | async-start | bytes 1572864 | tf_op jit(solution)/shard_map/all_gather | solution.py:132
  7.3 117.4 %all-gather.11.cloned.1.call-start = ((), (), s32[]{:S(2)}) async-start(), calls=%async_computation.2 | async-start | bytes 2621440 | tf_op jit(solution)/shard_map/all_gather | solution.py:145
  8.0 61.1 %copy-start.9 = (bf16[512,512]{1,0:T(8,128)(2,1)S(1)}, bf16[512,512]{1,0:T(8,128)(2,1)}, u32[]{:S(2)}) copy-start(bf16[512,512]{1,0:T(8,128)(2,1)} %param.20) | copy-start | bytes 1572868
  8.0 130.3 %all-gather.13.cloned.1.call-start = ((), (), s32[]{:S(2)}) async-start(), calls=%async_computation.3 | async-start | bytes 2621440 | tf_op jit(solution)/shard_map/all_gather | solution.py:146
  8.8 175.5 %all-gather.15.cloned.1.call-start = ((), (), s32[]{:S(2)}) async-start(), calls=%async_computation.4 | async-start | bytes 2621440 | tf_op jit(solution)/shard_map/all_gather | solution.py:147
  8.8 82.4 %collective-permute-start = (bf16[512,512]{1,0:T(8,128)(2,1)}, bf16[512,512]{1,0:T(8,128)(2,1)S(1)}, u32[]{:S(2)}, u32[]{:S(2)}) collective-permute-start(bf16[512,512]{1,0:T(8,128)(2,1)} %param.20), channel_id=1, source_target_pairs={{0,8},{8,16},{16,24},{24,0},{1,9},{9,17},{17,25},{25,1},{2,10},{10... | collective-permute-start | bytes 1572872 | tf_op jit(solution)/shard_map/ppermute | solution.py:24
  11.9 81.1 %collective-permute-start.1 = (bf16[512,512]{1,0:T(8,128)(2,1)}, bf16[512,512]{1,0:T(8,128)(2,1)}, u32[]{:S(2)}, u32[]{:S(2)}) collective-permute-start(bf16[512,512]{1,0:T(8,128)(2,1)} %param.20), channel_id=1, source_target_pairs={{0,24},{8,0},{16,8},{24,16},{1,25},{9,1},{17,9},{25,17},{2,26},{10... | collective-permute-start | bytes 1572872 | tf_op jit(solution)/shard_map/ppermute | solution.py:29
  14.0 56.8 %copy-start.14 = (bf16[512,128]{1,0:T(8,128)(2,1)S(1)}, bf16[512,128]{1,0:T(8,128)(2,1)}, u32[]{:S(2)}) copy-start(bf16[512,128]{1,0:T(8,128)(2,1)} %param.25) | copy-start | bytes 393220
  14.1 199.1 %all-gather.19.cloned.1.call-start = ((), (), s32[]{:S(2)}) async-start(), calls=%async_computation.7 | async-start | bytes 1310720 | tf_op jit(solution)/shard_map/all_gather | solution.py:39
  66.8 23.2 %copy-start.18 = (f32[256]{0:T(256)S(1)}, f32[256]{0:T(256)}, u32[]{:S(2)}) copy-start(f32[256]{0:T(256)} %add_convert_fusion.1) | copy-start | bytes 3076
  91.2 22.1 %copy-start.22 = (f32[2048]{0:T(1024)S(1)}, f32[2048]{0:T(1024)}, u32[]{:S(2)}) copy-start(f32[2048]{0:T(1024)} %param.19) | copy-start | bytes 24580
  91.2 21.2 %collective-permute-start.2 = (bf16[512,512]{1,0:T(8,128)(2,1)S(1)}, bf16[512,512]{1,0:T(8,128)(2,1)S(1)}, u32[]{:S(2)}, u32[]{:S(2)}) collective-permute-start(bf16[512,512]{1,0:T(8,128)(2,1)S(1)} %collective-permute-done), channel_id=1, source_target_pairs={{0,8},{8,16},{16,24},{24,0},{1,9},{9,17},{17,25},{25,1},{2,10},{10... | collective-permute-start | bytes 1572872 | tf_op jit(solution)/shard_map/ppermute | solution.py:24
  95.0 18.3 %copy-start.5 = (bf16[1,256,2048]{2,1,0:T(8,128)(2,1)S(1)}, bf16[1,256,2048]{2,1,0:T(8,128)(2,1)}, u32[]{:S(2)}) copy-start(bf16[1,256,2048]{2,1,0:T(8,128)(2,1)} %all-gather.17.cloned.1.call-done) | copy-start | bytes 3145732
  96.7 41.7 %copy-start.20 = (f32[256]{0:T(256)}, f32[256]{0:T(256)S(1)}, u32[]{:S(2)}) copy-start(f32[256]{0:T(256)S(1)} %add_rsqrt_fusion.1) | copy-start | bytes 3076
  117.7 9.7 %copy-start.11 = (bf16[256,128]{1,0:T(8,128)(2,1)}, bf16[256,128]{1,0:T(8,128)(2,1)S(1)}, u32[]{:S(2)}) copy-start(bf16[256,128]{1,0:T(8,128)(2,1)S(1)} %convolution_convert_fusion.5) | copy-start | bytes 196612
  118.3 36.9 %collective-permute-start.4 = (bf16[128,128]{1,0:T(8,128)(2,1)}, bf16[128,128]{1,0:T(8,128)(2,1)}, u32[]{:S(2)}, u32[]{:S(2)}) collective-permute-start(bf16[128,128]{1,0:T(8,128)(2,1)} %slice.64), channel_id=1, source_target_pairs={{0,8},{8,16},{16,24},{1,9},{9,17},{17,25},{2,10},{10,18},{18,26},{... | collective-permute-start | bytes 98312 | tf_op jit(solution)/shard_map/ppermute | solution.py:62
  151.1 103.6 %all-gather.21.cloned.1.call-start = ((), (), s32[]{:S(2)}) async-start(), calls=%async_computation.8 | async-start | bytes 2621440 | tf_op jit(solution)/shard_map/all_gather | solution.py:230
  153.1 31.2 %copy-start.6 = (bf16[1,256,2048]{2,1,0:T(8,128)(2,1)S(1)}, bf16[1,256,2048]{2,1,0:T(8,128)(2,1)}, u32[]{:S(2)}) copy-start(bf16[1,256,2048]{2,1,0:T(8,128)(2,1)} %all-gather.17.cloned.1.call-done) | copy-start | bytes 3145732
  153.4 3.7 %collective-permute-start.3 = (bf16[128,128]{1,0:T(8,128)(2,1)S(1)}, bf16[128,128]{1,0:T(8,128)(2,1)S(1)}, u32[]{:S(2)}, u32[]{:S(2)}) collective-permute-start(bf16[128,128]{1,0:T(8,128)(2,1)S(1)} %slice.63), channel_id=1, source_target_pairs={{0,8},{8,16},{16,24},{1,9},{9,17},{17,25},{2,10},{10,18},{18,26},{... | collective-permute-start | bytes 98312 | tf_op jit(solution)/shard_map/ppermute | solution.py:62
  159.0 27.9 %copy-start.15 = (pred[2,128,256]{1,2,0:T(8,128)(4,1)S(1)}, pred[2,128,256]{1,2,0:T(8,128)(4,1)}, u32[]{:S(2)}) copy-start(pred[2,128,256]{1,2,0:T(8,128)(4,1)} %broadcast_and_fusion) | copy-start | bytes 196612
  220.2 65.2 %reduce-scatter.2.cloned.1.call-start = ((), (), s32[]{:S(2)}) async-start(), calls=%async_computation.5 | async-start | bytes 1572864 | tf_op jit(solution)/shard_map/reduce_scatter | solution.py:239
  (14 other events, 55.0 us)
Sparse Core Ops, SparseCore 0:
  8.9 11.7 all-gather.16
  22.3 64.3 all-gather.10
  88.2 50.0 all-gather.12
  139.8 44.5 all-gather.14
  185.7 27.4 all-gather.18
  220.3 34.4 all-gather.20
  277.5 7.8 reduce-scatter.1
